TPU v7x, 32 devices: a whole 2x2x4 slice. The times are simulated.
32 devices in a mesh: grp: 2 (over y), fs: 4 (over z), tp: 4 (over x, core).
Axes of the slice: x: 2, y: 2, z: 4, core: 2. Of those that a mesh axis runs over, the one named last changes fastest.
Arguments:
- tokens: bfloat16 [6144, 2048], P(('grp', 'fs'), 'tp'), parts along dimension 0, may hold values from -6 to 6
- mix_gain: float32 [2048], replicated, may hold values from 0.1 to 1.9
- w_u: float32 [2048, 1024], P('fs', 'tp'), may hold values from -0.125 to 0.125
- w_v: float32 [2048, 1024], P('fs', 'tp'), may hold values from -0.125 to 0.125
- u_scale: float32 [1024], P('tp'), may hold values from 0.5 to 2
- v_scale: float32 [1024], P('tp'), may hold values from 0.5 to 2
- spatial: bfloat16 [8, 128, 128], P('tp'), may hold values from -0.5 to 0.5
- spatial_bias: float32 [8, 128], P('tp'), may hold values from 0.1 to 1.9
- w_mix: float32 [1024, 2048], P('tp', 'fs'), may hold values from -0.1875 to 0.1875
- mix_scale: float32 [1, 2048], P(None, 'fs'), may hold values from 0.5 to 2
- ffn_gain: float32 [2048], replicated, may hold values from 0.1 to 1.9
- w_gate: float32 [2048, 5632], P('fs', 'tp'), may hold values from -0.125 to 0.125
- w_up: float32 [2048, 5632], P('fs', 'tp'), may hold values from -0.125 to 0.125
- gate_scale: float32 [5632], P('tp'), may hold values from 0.5 to 2
- up_scale: float32 [5632], P('tp'), may hold values from 0.5 to 2
- w_down: float32 [5632, 2048], P('tp', 'fs'), may hold values from -0.078125 to 0.078125
- down_scale: float32 [1, 2048], P(None, 'fs'), may hold values from 0.5 to 2
Outputs:
- layer_out: bfloat16 [6144, 2048], P(('grp', 'fs'), 'tp'), parts along dimension 0
There are 2 independent parts, one for each index of `grp`. A program takes and returns all parts, laid end to end along the dimension named above; an argument that names none is the same for every part. Nothing has to cross between parts.
All inputs are finite; a program needn't handle non-finite values.
Results may differ from a plain program's by a relative error of at most 0.024.
Values may be sent and summed in bfloat16 or wider, within the bound.
A program may use at most 128 MiB of HBM per device.

v0:
```python
import jax
import jax.numpy as jnp
from jax import lax
from jax.sharding import PartitionSpec as P

eps = 1e-06


def norm_rows(shard, gain):
    whole = lax.all_gather(shard, "tp", axis=1, tiled=True)
    wide = whole.astype(jnp.float32)
    factor = lax.rsqrt(jnp.mean(wide * wide, axis=1, keepdims=True) + eps)
    return (wide * factor * gain).astype(jnp.bfloat16)


def project_pair(rows, first, second):
    left = first.astype(jnp.bfloat16)
    right = second.astype(jnp.bfloat16)
    return (
        jnp.dot(
            rows, lax.all_gather(left, "fs", axis=0, tiled=True), preferred_element_type=jnp.float32
        ),
        jnp.dot(
            rows,
            lax.all_gather(right, "fs", axis=0, tiled=True),
            preferred_element_type=jnp.float32,
        ),
    )


def collect_out(weight, scale):
    return (
        lax.all_gather(weight.astype(jnp.bfloat16), "fs", axis=1, tiled=True),
        lax.all_gather(scale.astype(jnp.bfloat16), "fs", axis=1, tiled=True).astype(scale.dtype),
    )


def reduce_out(hidden, weight, scale):
    term = jnp.dot(hidden, weight, preferred_element_type=jnp.float32) * scale
    return lax.psum_scatter(
        term.astype(jnp.bfloat16), "tp", scatter_dimension=1, tiled=True
    ).astype(jnp.float32)


def local(
    tokens,
    mix_gain,
    w_u,
    w_v,
    u_scale,
    v_scale,
    spatial,
    spatial_bias,
    w_mix,
    mix_scale,
    ffn_gain,
    w_gate,
    w_up,
    gate_scale,
    up_scale,
    w_down,
    down_scale,
):
    held = collect_out(w_mix, mix_scale)
    normed_in = norm_rows(tokens, mix_gain)
    u_pre, v_pre = project_pair(normed_in, w_u, w_v)
    u_act = jax.nn.gelu(u_pre * u_scale, approximate=False)
    v_act = jax.nn.gelu(v_pre * v_scale, approximate=False).astype(jnp.bfloat16)
    groups = spatial.shape[0]
    span = spatial.shape[1]
    count = v_act.shape[0]
    blocks = v_act.reshape(count // span, span, groups, v_act.shape[1] // groups)
    later = lax.broadcasted_iota(jnp.int32, (span, span), 0)
    earlier = lax.broadcasted_iota(jnp.int32, (span, span), 1)
    masked = jnp.where((later >= earlier)[None], spatial, jnp.zeros((), jnp.bfloat16))
    spatial_out = jnp.einsum("gts,nsgc->ntgc", masked, blocks, preferred_element_type=jnp.float32)
    spatial_out = spatial_out + spatial_bias.T[None, :, :, None]
    gated = (u_act * spatial_out.reshape(count, v_act.shape[1])).astype(jnp.bfloat16)
    mixed = reduce_out(gated, held[0], held[1])
    resid = (tokens.astype(jnp.float32) + mixed).astype(jnp.bfloat16)
    down_weight, down_factor = collect_out(w_down, down_scale)
    normed_ffn = norm_rows(resid, ffn_gain)
    gate_pre, up_pre = project_pair(normed_ffn, w_gate, w_up)
    act = (jax.nn.silu(gate_pre * gate_scale) * (up_pre * up_scale)).astype(jnp.bfloat16)
    down_sum = reduce_out(act, down_weight, down_factor)
    return (resid.astype(jnp.float32) + down_sum).astype(jnp.bfloat16)


def solution(mesh):
    placed = (
        P(("grp", "fs"), "tp"),
        P(),
        P("fs", "tp"),
        P("fs", "tp"),
        P("tp"),
        P("tp"),
        P("tp", None, None),
        P("tp", None),
        P("tp", "fs"),
        P(None, "fs"),
        P(),
        P("fs", "tp"),
        P("fs", "tp"),
        P("tp"),
        P("tp"),
        P("tp", "fs"),
        P(None, "fs"),
    )
    return jax.shard_map(
        local, mesh=mesh, in_specs=placed, out_specs=P(("grp", "fs"), "tp"), check_vma=False
    )
```

profile of v0, /device:TPU:0, one launch (start us, length us, event | category | flops | bytes accessed | tf_op | source)
XLA Modules:
  0.0 588.0 jit_solution(11109530156403825298)
XLA Ops:
  6.5 0.7 all-gather.9.cloned.1.call-update
  7.3 1.8 convert_element_type.75
  9.2 1.8 convert_element_type.74
  11.0 1.8 convert_element_type.78
  12.9 0.7 convert_element_type.79
  13.6 13.6 %all_gather.34 = bf16[1,2048]{1,0:T(2,128)(2,1)S(1)} all-gather(bf16[1,512]{1,0:T(2,128)(2,1)S(1)} %convert_element_type.79), channel_id=1, replica_groups=mesh['grp'=2,'fs'=4,'tp'=4] {'fs'}, dimensions={1}, use_global_device_ids=true | all-gather | bytes 5120 | tf_op jit(solution)/shard_map/all_gather | solution.py:34
  27.2 0.6 mul.159
  27.8 12.4 %all-gather.9.cloned.1.call-done = bf16[768,2048]{1,0:T(8,128)(2,1)} async-done(((bf16[768,512]{1,0:T(8,128)(2,1)}), bf16[768,2048]{1,0:T(8,128)(2,1)}) %all-gather.9.cloned.1.call-update) | async-done | bytes 3145744 | tf_op jit(solution)/shard_map/all_gather | solution.py:10
  40.2 2.6 fusion
  42.8 27.0 %all-gather.13.cloned.1.call-done = bf16[2048,256]{1,0:T(8,128)(2,1)} async-done(((bf16[512,256]{1,0:T(8,128)(2,1)}), bf16[2048,256]{1,0:T(8,128)(2,1)}) %all-gather.13.cloned.1.call-update) | async-done | bytes 1048592 | tf_op jit(solution)/shard_map/all_gather | solution.py:25
  69.8 5.5 fusion.20
  75.3 1.1 reshape.36
  76.4 2.0 fusion.6
  78.4 2.1 copy.19
  80.5 18.2 %all-gather.11.cloned.1.call-done = bf16[2048,256]{1,0:T(8,128)(2,1)} async-done(((bf16[512,256]{1,0:T(8,128)(2,1)}), bf16[2048,256]{1,0:T(8,128)(2,1)}) %all-gather.11.cloned.1.call-update) | async-done | bytes 1048592 | tf_op jit(solution)/shard_map/all_gather | solution.py:21
  98.7 28.8 %all-gather.15.cloned.1.call-done = bf16[256,2048]{1,0:T(8,128)(2,1)} async-done(((bf16[256,512]{1,0:T(8,128)(2,1)}), bf16[256,2048]{1,0:T(8,128)(2,1)}) %all-gather.15.cloned.1.call-update) | async-done | bytes 1048592 | tf_op jit(solution)/shard_map/all_gather | solution.py:33
  127.5 8.4 %multiply_convert_fusion.1 = bf16[768,2048]{1,0:T(8,128)(2,1)} fusion(bf16[256,2048]{1,0:T(8,128)(2,1)} %all-gather.15.cloned.1.call-done, f32[2048]{0:T(1024)} %bitcast.25, f32[96,8,2,128]{3,2,1,0:T(2,128)} %bitcast.24, bf16[2048,256]{1,0:T(8,128)(2,1)} %all-gather.11.cloned.1.call-done, bf16[768,2048]{1,0:T(8,128)(2,1)S(1)} %copy-done.1, ...), kind=kOutput, calls=%fused_computation.11 | convolution fusion | flops 1633222656 | bytes 9195520 | tf_op jit(solution)/shard_map/dot_general | solution.py:39
  136.0 37.2 %reduce-scatter.3.cloned.1.call-done = bf16[768,512]{1,0:T(8,128)(2,1)} async-done(((bf16[768,2048]{1,0:T(8,128)(2,1)}), bf16[768,512]{1,0:T(8,128)(2,1)}) %reduce-scatter.3.cloned.1.call-update) | async-done | bytes 786448 | tf_op jit(solution)/shard_map/reduce_scatter | solution.py:40
  173.2 2.5 add_convert_fusion.1
  175.8 1.3 convert_element_type.86
  177.1 3.3 convert_element_type.87
  180.5 1.3 convert_element_type.89
  181.9 12.2 %all_gather.39 = bf16[1,2048]{1,0:T(2,128)(2,1)S(1)} all-gather(bf16[1,512]{1,0:T(2,128)(2,1)S(1)} %convert_element_type.90), channel_id=1, replica_groups=mesh['grp'=2,'fs'=4,'tp'=4] {'fs'}, dimensions={1}, use_global_device_ids=true | all-gather | bytes 5120 | tf_op jit(solution)/shard_map/all_gather | solution.py:34
  194.1 10.3 %all-gather.17.cloned.1.call-done = bf16[768,2048]{1,0:T(8,128)(2,1)} async-done(((bf16[768,512]{1,0:T(8,128)(2,1)}), bf16[768,2048]{1,0:T(8,128)(2,1)}) %all-gather.17.cloned.1.call-update) | async-done | bytes 3145744 | tf_op jit(solution)/shard_map/all_gather | solution.py:10
  204.4 2.6 fusion.3
  207.0 105.7 %all-gather.19.cloned.1.call-done = bf16[2048,1408]{1,0:T(8,128)(2,1)} async-done(((bf16[512,1408]{1,0:T(8,128)(2,1)}), bf16[2048,1408]{1,0:T(8,128)(2,1)}) %all-gather.19.cloned.1.call-update) | async-done | bytes 5767184 | tf_op jit(solution)/shard_map/all_gather | solution.py:21
  312.7 9.9 %fusion.8 = f32[768,1408]{1,0:T(8,128)} fusion(bf16[2048,1408]{1,0:T(8,128)(2,1)} %all-gather.19.cloned.1.call-done, bf16[768,2048]{1,0:T(8,128)(2,1)} %all-gather.17.cloned.1.call-done, f32[2048]{0:T(1024)S(1)} %copy-done.7, f32[768]{0:T(1024)S(1)} %add_rsqrt_fusion), kind=kOutput, calls=%fused_computation.21 | convolution fusion | flops 4435476480 | bytes 13249536 | tf_op jit(solution)/shard_map/dot_general | solution.py:20
  322.6 96.6 %all-gather.21.cloned.1.call-done = bf16[2048,1408]{1,0:T(8,128)(2,1)} async-done(((bf16[512,1408]{1,0:T(8,128)(2,1)}), bf16[2048,1408]{1,0:T(8,128)(2,1)}) %all-gather.21.cloned.1.call-update) | async-done | bytes 5767184 | tf_op jit(solution)/shard_map/all_gather | solution.py:25
  419.2 106.5 %all-gather.23.cloned.1.call-done = bf16[1408,2048]{1,0:T(8,128)(2,1)} async-done(((bf16[1408,512]{1,0:T(8,128)(2,1)}), bf16[1408,2048]{1,0:T(8,128)(2,1)}) %all-gather.23.cloned.1.call-update) | async-done | bytes 5767184 | tf_op jit(solution)/shard_map/all_gather | solution.py:33
  525.8 17.1 %multiply_convert_fusion = bf16[768,2048]{1,0:T(8,128)(2,1)} fusion(bf16[1408,2048]{1,0:T(8,128)(2,1)} %all-gather.23.cloned.1.call-done, f32[2048]{0:T(1024)S(1)} %bitcast.26, f32[768,1408]{1,0:T(8,128)} %fusion.8, bf16[2048,1408]{1,0:T(8,128)(2,1)} %all-gather.21.cloned.1.call-done, f32[1408]{0:T(1024)S(1)} %copy-done.8, f32[1408]{0:T(1024)S(1)} %copy-done.9, ...), kind=kOutput, calls=%fused_computation.10 | convolution fusion | flops 8876457984 | bytes 22181888 | tf_op jit(solution)/shard_map/dot_general | solution.py:39
  542.9 36.1 %reduce-scatter.5.cloned.1.call-done = bf16[768,512]{1,0:T(8,128)(2,1)} async-done(((bf16[768,2048]{1,0:T(8,128)(2,1)}), bf16[768,512]{1,0:T(8,128)(2,1)}) %reduce-scatter.5.cloned.1.call-update) | async-done | bytes 786448 | tf_op jit(solution)/shard_map/reduce_scatter | solution.py:40
  579.0 2.2 add_convert_fusion
  (46 shorter events, 0.6 us)
Async XLA Ops:
  6.5 63.2 %copy-start.6 = (f32[2048]{0:T(1024)S(1)}, f32[2048]{0:T(1024)}, u32[]{:S(2)}) copy-start(f32[2048]{0:T(1024)} %param.18) | copy-start | bytes 24580
  6.5 63.2 %copy-start.10 = (f32[256]{0:T(256)S(1)}, f32[256]{0:T(256)}, u32[]{:S(2)}) copy-start(f32[256]{0:T(256)} %param.22) | copy-start | bytes 3076
  6.5 33.6 %all-gather.9.cloned.1.call-start = ((), (), s32[]{:S(2)}) async-start(), calls=%async_computation.2 | async-start | bytes 3932160 | tf_op jit(solution)/shard_map/all_gather | solution.py:10
  7.3 62.5 %all-gather.13.cloned.1.call-start = ((), (), s32[]{:S(2)}) async-start(), calls=%async_computation.4 | async-start | bytes 1310720 | tf_op jit(solution)/shard_map/all_gather | solution.py:25
  9.1 89.6 %all-gather.11.cloned.1.call-start = ((), (), s32[]{:S(2)}) async-start(), calls=%async_computation.3 | async-start | bytes 1310720 | tf_op jit(solution)/shard_map/all_gather | solution.py:21
  11.0 116.6 %all-gather.15.cloned.1.call-start = ((), (), s32[]{:S(2)}) async-start(), calls=%async_computation.5 | async-start | bytes 1310720 | tf_op jit(solution)/shard_map/all_gather | solution.py:33
  12.8 160.4 %reduce-scatter.3.cloned.1.call-start = ((), (), s32[]{:S(2)}) async-start(), calls=%async_computation.6 | async-start | bytes 3932160 | tf_op jit(solution)/shard_map/reduce_scatter | solution.py:40
  42.7 27.0 %copy-start.4 = (f32[768]{0:T(1024)}, f32[768]{0:T(1024)S(1)}, u32[]{:S(2)}) copy-start(f32[768]{0:T(1024)S(1)} %add_rsqrt_fusion.1) | copy-start | bytes 9220
  42.8 84.8 %copy-start.1 = (bf16[768,2048]{1,0:T(8,128)(2,1)S(1)}, bf16[768,2048]{1,0:T(8,128)(2,1)}, u32[]{:S(2)}) copy-start(bf16[768,2048]{1,0:T(8,128)(2,1)} %all-gather.9.cloned.1.call-done) | copy-start | bytes 9437188
  136.0 39.8 %copy-start.2 = (f32[512,1408]{1,0:T(8,128)S(1)}, f32[512,1408]{1,0:T(8,128)}, u32[]{:S(2)}) copy-start(f32[512,1408]{1,0:T(8,128)} %param.28) | copy-start | bytes 8650756
  136.0 68.4 %all-gather.17.cloned.1.call-start = ((), (), s32[]{:S(2)}) async-start(), calls=%async_computation.7 | async-start | bytes 3932160 | tf_op jit(solution)/shard_map/all_gather | solution.py:10
  175.7 137.0 %all-gather.19.cloned.1.call-start = ((), (), s32[]{:S(2)}) async-start(), calls=%async_computation.8 | async-start | bytes 7208960 | tf_op jit(solution)/shard_map/all_gather | solution.py:21
  177.0 3.5 copy-start.3
  177.1 242.1 %all-gather.21.cloned.1.call-start = ((), (), s32[]{:S(2)}) async-start(), calls=%async_computation.9 | async-start | bytes 7208960 | tf_op jit(solution)/shard_map/all_gather | solution.py:25
  180.4 1.5 copy-start.5
  180.4 132.2 %copy-start.7 = (f32[2048]{0:T(1024)S(1)}, f32[2048]{0:T(1024)}, u32[]{:S(2)}) copy-start(f32[2048]{0:T(1024)} %param.27) | copy-start | bytes 24580
  180.4 345.3 %all-gather.23.cloned.1.call-start = ((), (), s32[]{:S(2)}) async-start(), calls=%async_computation.10 | async-start | bytes 7208960 | tf_op jit(solution)/shard_map/all_gather | solution.py:33
  181.8 397.2 %reduce-scatter.5.cloned.1.call-start = ((), (), s32[]{:S(2)}) async-start(), calls=%async_computation.11 | async-start | bytes 3932160 | tf_op jit(solution)/shard_map/reduce_scatter | solution.py:40
  206.9 318.8 %copy-start.8 = (f32[1408]{0:T(1024)S(1)}, f32[1408]{0:T(1024)}, u32[]{:S(2)}) copy-start(f32[1408]{0:T(1024)} %param.31) | copy-start | bytes 16900
  207.0 318.8 %copy-start.9 = (f32[1408]{0:T(1024)S(1)}, f32[1408]{0:T(1024)}, u32[]{:S(2)}) copy-start(f32[1408]{0:T(1024)} %param.30) | copy-start | bytes 16900
  525.8 53.2 %copy-start = (bf16[768,512]{1,0:T(8,128)(2,1)S(1)}, bf16[768,512]{1,0:T(8,128)(2,1)}, u32[]{:S(2)}) copy-start(bf16[768,512]{1,0:T(8,128)(2,1)} %add_convert_fusion.1) | copy-start | bytes 2359300
Sparse Core Ops, SparseCore 0:
  8.9 31.2 all-gather.8
  41.7 27.9 all-gather.12
  71.3 27.3 all-gather.10
  100.1 27.3 all-gather.14
  136.1 37.0 reduce-scatter.2
  175.8 28.5 all-gather.16
  205.9 106.6 all-gather.18
  314.2 104.9 all-gather.20
  420.8 104.9 all-gather.22
  543.0 35.9 reduce-scatter.4
where the time goes:
time: 589 us; the launch traced here: 588 us
  waiting for transfers between devices  480 us (81%)
  matrix products  43 us (7%)
  blocking collectives  25.8 us (4%)
  other arithmetic  22.3 us (4%)
  between operations  13.6 us (2%)
    all_gather x2, waiting for transfers between devices, collect_out(): lax.all_gather(weight.astype(jnp.bfloat16), 'fs', axis=1, tiled=True)  135 us
    all_gather x2, waiting for transfers between devices, project_pair(): lax.all_gather(left, 'fs', axis=0, tiled=True)  124 us
    all_gather x2, waiting for transfers between devices, project_pair(): lax.all_gather(right, 'fs', axis=0, tiled=True)  124 us
    reduce_scatter x2, waiting for transfers between devices, reduce_out(): lax.psum_scatter(term.astype(jnp.bfloat16), 'tp', scatter_dimension=1, ti...  73.3 us
    all_gather x2, blocking collectives, collect_out(): lax.all_gather(scale.astype(jnp.bfloat16), 'fs', axis=1, tiled=True)  25.8 us
    dot_general x2, matrix products, reduce_out(): term = jnp.dot(hidden, weight, preferred_element_type=jnp.float32) * scale  25.5 us
    all_gather x2, waiting for transfers between devices, norm_rows(): whole = lax.all_gather(shard, 'tp', axis=1, tiled=True)  22.7 us
  transfers between devices with their start and end apart: 10, of which 10 were waited for; matrix products, arithmetic and copies ran while one was open for 7% of the time, Pallas kernels for 0%

commit v1 on v0

--- a/solution.py
+++ b/solution.py
@@ -13,25 +13,25 @@
     return (wide * factor * gain).astype(jnp.bfloat16)
 
 
-def project_pair(rows, first, second):
-    left = first.astype(jnp.bfloat16)
-    right = second.astype(jnp.bfloat16)
-    return (
-        jnp.dot(
-            rows, lax.all_gather(left, "fs", axis=0, tiled=True), preferred_element_type=jnp.float32
-        ),
-        jnp.dot(
-            rows,
-            lax.all_gather(right, "fs", axis=0, tiled=True),
-            preferred_element_type=jnp.float32,
-        ),
-    )
+def swap_gather(weight, axis):
+    groups = lax.axis_size("grp")
+    half = weight.shape[0] // groups
+    mine = lax.axis_index("grp")
+    piece = lax.dynamic_slice_in_dim(weight, mine * half, half, 0).astype(jnp.bfloat16)
+    held = lax.all_gather(piece, "fs", axis=0)
+    other = lax.ppermute(held, "grp", [(i, (i + 1) % groups) for i in range(groups)])
+    first = jnp.where(mine == 0, held, other)
+    second = jnp.where(mine == 0, other, held)
+    whole = jnp.concatenate([first, second], axis=1)
+    if axis == 0:
+        return whole.reshape(-1, weight.shape[1])
+    return whole.transpose(1, 0, 2).reshape(weight.shape[0], -1)
 
 
-def collect_out(weight, scale):
+def project_pair(rows, first, second):
     return (
-        lax.all_gather(weight.astype(jnp.bfloat16), "fs", axis=1, tiled=True),
-        lax.all_gather(scale.astype(jnp.bfloat16), "fs", axis=1, tiled=True).astype(scale.dtype),
+        jnp.dot(rows, swap_gather(first, 0), preferred_element_type=jnp.float32),
+        jnp.dot(rows, swap_gather(second, 0), preferred_element_type=jnp.float32),
     )
 
 
@@ -61,7 +61,8 @@
     w_down,
     down_scale,
 ):
-    held = collect_out(w_mix, mix_scale)
+    scales = lax.all_gather(jnp.concatenate([mix_scale, down_scale], axis=0), "fs", axis=1, tiled=True)
+    held = (swap_gather(w_mix, 1), scales[:1])
     normed_in = norm_rows(tokens, mix_gain)
     u_pre, v_pre = project_pair(normed_in, w_u, w_v)
     u_act = jax.nn.gelu(u_pre * u_scale, approximate=False)
@@ -78,7 +79,7 @@
     gated = (u_act * spatial_out.reshape(count, v_act.shape[1])).astype(jnp.bfloat16)
     mixed = reduce_out(gated, held[0], held[1])
     resid = (tokens.astype(jnp.float32) + mixed).astype(jnp.bfloat16)
-    down_weight, down_factor = collect_out(w_down, down_scale)
+    down_weight, down_factor = swap_gather(w_down, 1), scales[1:]
     normed_ffn = norm_rows(resid, ffn_gain)
     gate_pre, up_pre = project_pair(normed_ffn, w_gate, w_up)
     act = (jax.nn.silu(gate_pre * gate_scale) * (up_pre * up_scale)).astype(jnp.bfloat16)

time: 589 us -> 411 us (0.70)
  waiting for transfers between devices: 480 us -> 231 us
  blocking collectives: 25.8 us -> 68.5 us
  local copies, waits for them, and re-layouts: 3.27 us -> 20.8 us
  other arithmetic: 22.3 us -> 30 us
  starting transfers between devices: 0.38 us -> 7.57 us
    all_gather x6 -> x3, waiting for transfers between devices: 383 us -> 113 us  [swap_gather(): held = lax.all_gather(piece, 'fs', axis=0)]
    all_gather x2 -> x4, blocking collectives: 25.8 us -> 68.5 us  [the longest x3 54.7 us: swap_gather(): held = lax.all_gather(piece, 'fs', axis=0)]
    ppermute x0 -> x6, waiting for transfers between devices: none -> 42.4 us  [swap_gather(): lax.ppermute(held, 'grp', [(i, (i + 1) % groups) for i in range(groups)])]
    all_gather x2, waiting for transfers between devices: 22.7 us -> 0.02 us  [norm_rows(): whole = lax.all_gather(shard, 'tp', axis=1, tiled=True)]
    convert_element_type x8 -> x0, other arithmetic: 11.9 us -> none  [the longest x2 5.07 us: project_pair(): right = second.astype(jnp.bfloat16)]
    select_n x0 -> x6, other arithmetic: none -> 9.99 us  [swap_gather(): first = jnp.where(mine == 0, held, other)]
    transpose x0 -> x2, local copies, waits for them, and re-layouts: none -> 9.68 us  [swap_gather(): return whole.transpose(1, 0, 2).reshape(weight.shape[0], -1)]
    convert_element_type x0 -> x6, local copies, waits for them, and re-layouts: none -> 8.52 us  [swap_gather(): lax.dynamic_slice_in_dim(weight, mine * half, half, 0).astype(jnp.bfloat16)]
  transfers between devices with their start and end apart: 10 -> 13, of which waited for: 10 -> 5; matrix products, arithmetic and copies ran while one was open for 7% -> 14% of each run, Pallas kernels for 0% -> 0%
where the time goes in v1:
time: 411 us; the launch traced here: 410 us
  waiting for transfers between devices  231 us (56%)
  blocking collectives  68.5 us (17%)
  matrix products  38.9 us (9%)
  other arithmetic  30 us (7%)
  local copies, waits for them, and re-layouts  20.8 us (5%)
  between operations  13.8 us (3%)
  starting transfers between devices  7.57 us (2%)
    all_gather x3, waiting for transfers between devices, swap_gather(): held = lax.all_gather(piece, 'fs', axis=0)  113 us
    reduce_scatter x2, waiting for transfers between devices, reduce_out(): lax.psum_scatter(term.astype(jnp.bfloat16), 'tp', scatter_dimension=1, ti...  74.1 us
    all_gather x3, blocking collectives, swap_gather(): held = lax.all_gather(piece, 'fs', axis=0)  54.7 us
    ppermute x6, waiting for transfers between devices, swap_gather(): lax.ppermute(held, 'grp', [(i, (i + 1) % groups) for i in range(groups)])  42.4 us
    dot_general x2, matrix products, reduce_out(): term = jnp.dot(hidden, weight, preferred_element_type=jnp.float32) * scale  26.3 us
    all_gather x1, blocking collectives, local(): lax.all_gather(jnp.concatenate([mix_scale, down_scale], axis=0), 'fs', ax...  13.8 us
    select_n x6, other arithmetic, swap_gather(): first = jnp.where(mine == 0, held, other)  9.99 us
    transpose x2, local copies, waits for them, and re-layouts, swap_gather(): return whole.transpose(1, 0, 2).reshape(weight.shape[0], -1)  9.68 us
  transfers between devices with their start and end apart: 13, of which 5 were waited for; matrix products, arithmetic and copies ran while one was open for 14% of the time, Pallas kernels for 0%

profile of v1, /device:TPU:0, one launch (start us, length us, event | category | flops | bytes accessed | tf_op | source)
XLA Modules:
  0.0 410.3 jit_solution(16910831482225574625)
XLA Ops:
  10.4 17.4 %all-gather.2 = bf16[512,512]{1,0:T(8,128)(2,1)S(1)} all-gather(bf16[128,512]{1,0:T(8,128)(2,1)S(1)} %dynamic-slice_convert_fusion.3), channel_id=4, replica_groups=mesh['grp'=2,'fs'=4,'tp'=4] {'fs'}, dimensions={0}, use_global_device_ids=true | all-gather | bytes 655360 | tf_op jit(solution)/shard_map/all_gather | solution.py:21
  27.8 1.5 collective-permute-start.2
  30.2 16.2 %all-gather = bf16[1024,256]{1,0:T(8,128)(2,1)S(1)} all-gather(bf16[256,256]{1,0:T(8,128)(2,1)S(1)} %dynamic-slice_convert_fusion.5), channel_id=2, replica_groups=mesh['grp'=2,'fs'=4,'tp'=4] {'fs'}, dimensions={0}, use_global_device_ids=true | all-gather | bytes 655360 | tf_op jit(solution)/shard_map/all_gather | solution.py:21
  47.9 21.1 %all-gather.1 = bf16[1024,256]{1,0:T(8,128)(2,1)S(1)} all-gather(bf16[256,256]{1,0:T(8,128)(2,1)S(1)} %dynamic-slice_convert_fusion.4), channel_id=3, replica_groups=mesh['grp'=2,'fs'=4,'tp'=4] {'fs'}, dimensions={0}, use_global_device_ids=true | all-gather | bytes 655360 | tf_op jit(solution)/shard_map/all_gather | solution.py:21
  69.0 1.5 collective-permute-start.1
  70.5 2.3 dynamic-slice_convert_fusion.1
  72.9 13.8 %all_gather.52 = f32[2,2048]{1,0:T(2,128)S(1)} all-gather(f32[2,512]{1,0:T(2,128)S(1)} %pad_maximum_fusion.4), channel_id=1, replica_groups=mesh['grp'=2,'fs'=4,'tp'=4] {'fs'}, dimensions={1}, use_global_device_ids=true | all-gather | bytes 20480 | tf_op jit(solution)/shard_map/all_gather | solution.py:64
  86.9 1.3 copy.24
  90.6 2.7 fusion
  93.5 2.9 fusion.20
  96.9 1.2 copy.23
  98.1 9.1 %multiply_convert_fusion.1 = bf16[768,2048]{1,0:T(8,128)(2,1)} fusion(bf16[256,2048]{0,1:T(8,128)(2,1)S(1)} %bitcast.55, f32[2048]{0:T(1024)S(1)} %bitcast.60, f32[96,8,2,128]{3,2,1,0:T(2,128)} %bitcast.58, bf16[2048,256]{1,0:T(8,128)(2,1)} %bitcast.56, bf16[768,2048]{1,0:T(8,128)(2,1)} %all-gather.12.cloned.1.call-done, f32[2048]{0:T(1024)S(1)} %copy-done.11, ...), kind=kOutput, calls=%fused_computation.11 | convolution fusion | flops 1633222656 | bytes 9195520 | tf_op jit(solution)/shard_map/dot_general | solution.py:39
  107.2 2.4 dynamic-slice_convert_fusion.2
  110.4 55.2 %all-gather.18.cloned.1.call-done = bf16[1024,1408]{1,0:T(8,128)(2,1)} async-done(((bf16[256,1408]{1,0:T(8,128)(2,1)}), bf16[1024,1408]{1,0:T(8,128)(2,1)}) %all-gather.18.cloned.1.call-update) | async-done | bytes 2883600 | tf_op jit(solution)/shard_map/all_gather | solution.py:21
  165.6 1.5 collective-permute-start.4
  167.1 37.3 %reduce-scatter.3.cloned.1.call-done = bf16[768,512]{1,0:T(8,128)(2,1)} async-done(((bf16[768,2048]{1,0:T(8,128)(2,1)}), bf16[768,512]{1,0:T(8,128)(2,1)}) %reduce-scatter.3.cloned.1.call-update) | async-done | bytes 786448 | tf_op jit(solution)/shard_map/reduce_scatter | solution.py:40
  204.4 2.2 add_convert_fusion.1
  206.9 58.1 %all-gather.16.cloned.1.call-done = bf16[1024,1408]{1,0:T(8,128)(2,1)} async-done(((bf16[256,1408]{1,0:T(8,128)(2,1)}), bf16[1024,1408]{1,0:T(8,128)(2,1)}) %all-gather.16.cloned.1.call-update) | async-done | bytes 2883600 | tf_op jit(solution)/shard_map/all_gather | solution.py:21
  265.0 1.5 collective-permute-start.3
  266.5 3.1 broadcast_select_fusion.1
  269.5 2.9 maximum_bitcast_fusion
  272.4 8.4 %copy.25 = bf16[1408,4,512]{0,2,1:T(8,128)(2,1)} copy(bf16[1408,4,512]{2,0,1:T(8,128)(2,1)} %maximum_bitcast_fusion) | data formatting | bytes 11534336 | tf_op jit(solution)/shard_map/transpose | solution.py:28
  280.8 3.2 broadcast_select_fusion.3
  284.0 2.9 pad_maximum_fusion.1
  287.0 42.4 %collective-permute-done.3 = bf16[4,256,1408]{2,1,0:T(8,128)(2,1)} collective-permute-done((bf16[4,256,1408]{2,1,0:T(8,128)(2,1)}, bf16[4,256,1408]{2,1,0:T(8,128)(2,1)}, u32[]{:S(2)}, u32[]{:S(2)}) %collective-permute-start.3) | collective-permute-done | bytes 2883616 | tf_op jit(solution)/shard_map/ppermute | solution.py:22
  329.4 2.4 broadcast_select_fusion.5
  331.8 2.9 pad_maximum_fusion
  334.7 2.7 fusion.3
  337.5 9.5 %fusion.8 = f32[768,1408]{1,0:T(8,128)} fusion(bf16[2048,1408]{1,0:T(8,128)(2,1)} %bitcast.42, bf16[768,2048]{1,0:T(8,128)(2,1)S(1)} %copy-done.3, f32[2048]{0:T(1024)S(1)} %copy-done.12, f32[768]{0:T(1024)S(1)} %add_rsqrt_fusion), kind=kOutput, calls=%fused_computation.36 | convolution fusion | flops 4435476480 | bytes 13249536 | tf_op jit(solution)/shard_map/dot_general | solution.py:33
  347.0 17.2 %multiply_convert_fusion = bf16[768,2048]{1,0:T(8,128)(2,1)} fusion(bf16[1408,2048]{0,1:T(8,128)(2,1)} %bitcast.40, f32[2048]{0:T(1024)S(1)} %bitcast.59, f32[768,1408]{1,0:T(8,128)} %fusion.8, bf16[2048,1408]{1,0:T(8,128)(2,1)} %bitcast.41, f32[1408]{0:T(1024)S(1)} %copy-done.13, f32[1408]{0:T(1024)S(1)} %copy-done.14, ...), kind=kOutput, calls=%fused_computation.10 | convolution fusion | flops 8876457984 | bytes 22181888 | tf_op jit(solution)/shard_map/dot_general | solution.py:39
  364.2 36.8 %reduce-scatter.5.cloned.1.call-done = bf16[768,512]{1,0:T(8,128)(2,1)} async-done(((bf16[768,2048]{1,0:T(8,128)(2,1)}), bf16[768,512]{1,0:T(8,128)(2,1)}) %reduce-scatter.5.cloned.1.call-update) | async-done | bytes 786448 | tf_op jit(solution)/shard_map/reduce_scatter | solution.py:40
  400.9 2.5 add_convert_fusion
  (75 shorter events, 10.6 us)
Async XLA Ops:
  6.5 1.8 copy-start
  6.5 84.1 %all-gather.12.cloned.1.call-start = ((), (), s32[]{:S(2)}) async-start(), calls=%async_computation.2 | async-start | bytes 3932160 | tf_op jit(solution)/shard_map/all_gather | solution.py:10
  7.3 102.4 %all-gather.20.cloned.1.call-start = ((), (), s32[]{:S(2)}) async-start(), calls=%async_computation.8 | async-start | bytes 3604480 | tf_op jit(solution)/shard_map/all_gather | solution.py:21
  9.3 63.6 %copy-start.8 = (f32[1,512]{1,0:T(1,128)S(1)}, f32[1,512]{1,0:T(1,128)}, u32[]{:S(2)}) copy-start(f32[1,512]{1,0:T(1,128)} %param.33) | copy-start | bytes 6148
  9.3 63.6 %copy-start.9 = (f32[1,512]{1,0:T(1,128)S(1)}, f32[1,512]{1,0:T(1,128)}, u32[]{:S(2)}) copy-start(f32[1,512]{1,0:T(1,128)} %param.26) | copy-start | bytes 6148
  9.4 156.2 %all-gather.18.cloned.1.call-start = ((), (), s32[]{:S(2)}) async-start(), calls=%async_computation.7 | async-start | bytes 3604480 | tf_op jit(solution)/shard_map/all_gather | solution.py:21
  27.8 59.0 %collective-permute-start.2 = (bf16[4,128,512]{2,1,0:T(8,128)(2,1)S(1)}, bf16[4,128,512]{2,1,0:T(8,128)(2,1)S(1)}, u32[]{:S(2)}, u32[]{:S(2)}) collective-permute-start(bf16[4,128,512]{2,1,0:T(8,128)(2,1)S(1)} %bitcast.51), channel_id=1, source_target_pairs={{0,16},{16,0},{1,17},{17,1},{2,18},{18,2},{3,19},{19,3},{4,20},{20... | collective-permute-start | bytes 1572872 | tf_op jit(solution)/shard_map/ppermute | solution.py:22
  46.4 41.8 %collective-permute-start = (bf16[4,256,256]{2,1,0:T(8,128)(2,1)S(1)}, bf16[4,256,256]{2,1,0:T(8,128)(2,1)}, u32[]{:S(2)}, u32[]{:S(2)}) collective-permute-start(bf16[4,256,256]{2,1,0:T(8,128)(2,1)S(1)} %bitcast.53), channel_id=1, source_target_pairs={{0,16},{16,0},{1,17},{17,1},{2,18},{18,2},{3,19},{19,3},{4,20},{20... | collective-permute-start | bytes 1572872 | tf_op jit(solution)/shard_map/ppermute | solution.py:22
  69.0 21.4 %collective-permute-start.1 = (bf16[4,256,256]{2,1,0:T(8,128)(2,1)S(1)}, bf16[4,256,256]{2,1,0:T(8,128)(2,1)S(1)}, u32[]{:S(2)}, u32[]{:S(2)}) collective-permute-start(bf16[4,256,256]{2,1,0:T(8,128)(2,1)S(1)} %bitcast.49), channel_id=1, source_target_pairs={{0,16},{16,0},{1,17},{17,1},{2,18},{18,2},{3,19},{19,3},{4,20},{20... | collective-permute-start | bytes 1572872 | tf_op jit(solution)/shard_map/ppermute | solution.py:22
  72.8 131.6 %reduce-scatter.3.cloned.1.call-start = ((), (), s32[]{:S(2)}) async-start(), calls=%async_computation.3 | async-start | bytes 3932160 | tf_op jit(solution)/shard_map/reduce_scatter | solution.py:40
  90.5 2.9 copy-start.11
  90.5 2.9 copy-start.15
  90.6 2.9 copy-start.2
  93.5 3.1 copy-start.7
  93.5 3.1 copy-start.10
  96.4 1.6 copy-start.6
  96.4 1.6 copy-start.16
  107.1 97.3 %copy-start.4 = (bf16[768,512]{1,0:T(8,128)(2,1)S(1)}, bf16[768,512]{1,0:T(8,128)(2,1)}, u32[]{:S(2)}) copy-start(bf16[768,512]{1,0:T(8,128)(2,1)} %param.17) | copy-start | bytes 2359300
  107.2 157.8 %all-gather.16.cloned.1.call-start = ((), (), s32[]{:S(2)}) async-start(), calls=%async_computation.6 | async-start | bytes 3604480 | tf_op jit(solution)/shard_map/all_gather | solution.py:21
  109.6 225.1 %all-gather.14.cloned.1.call-start = ((), (), s32[]{:S(2)}) async-start(), calls=%async_computation.4 | async-start | bytes 3932160 | tf_op jit(solution)/shard_map/all_gather | solution.py:10
  109.7 156.8 %collective-permute-start.5 = (bf16[4,704,512]{2,1,0:T(8,128)(2,1)}, bf16[4,704,512]{2,1,0:T(8,128)(2,1)}, u32[]{:S(2)}, u32[]{:S(2)}) collective-permute-start(bf16[4,704,512]{2,1,0:T(8,128)(2,1)} %bitcast.43), channel_id=1, source_target_pairs={{0,16},{16,0},{1,17},{17,1},{2,18},{18,2},{3,19},{19,3},{4,20},{20... | collective-permute-start | bytes 8650760 | tf_op jit(solution)/shard_map/ppermute | solution.py:22
  165.6 115.2 %collective-permute-start.4 = (bf16[4,256,1408]{2,1,0:T(8,128)(2,1)}, bf16[4,256,1408]{2,1,0:T(8,128)(2,1)}, u32[]{:S(2)}, u32[]{:S(2)}) collective-permute-start(bf16[4,256,1408]{2,1,0:T(8,128)(2,1)} %bitcast.45), channel_id=1, source_target_pairs={{0,16},{16,0},{1,17},{17,1},{2,18},{18,2},{3,19},{19,3},{4,20},{20... | collective-permute-start | bytes 8650760 | tf_op jit(solution)/shard_map/ppermute | solution.py:22
  206.7 194.3 %reduce-scatter.5.cloned.1.call-start = ((), (), s32[]{:S(2)}) async-start(), calls=%async_computation.5 | async-start | bytes 3932160 | tf_op jit(solution)/shard_map/reduce_scatter | solution.py:40
  265.0 64.4 %collective-permute-start.3 = (bf16[4,256,1408]{2,1,0:T(8,128)(2,1)}, bf16[4,256,1408]{2,1,0:T(8,128)(2,1)}, u32[]{:S(2)}, u32[]{:S(2)}) collective-permute-start(bf16[4,256,1408]{2,1,0:T(8,128)(2,1)} %bitcast.47), channel_id=1, source_target_pairs={{0,16},{16,0},{1,17},{17,1},{2,18},{18,2},{3,19},{19,3},{4,20},{20... | collective-permute-start | bytes 8650760 | tf_op jit(solution)/shard_map/ppermute | solution.py:22
  284.0 45.3 %copy-start.5 = (bf16[1024,1408]{1,0:T(8,128)(2,1)S(1)}, bf16[1024,1408]{1,0:T(8,128)(2,1)}, u32[]{:S(2)}) copy-start(bf16[1024,1408]{1,0:T(8,128)(2,1)} %all-gather.16.cloned.1.call-done) | copy-start | bytes 8650756
  334.6 2.7 copy-start.12
  334.7 2.8 copy-start.3
  337.5 9.5 %copy-start.13 = (f32[1408]{0:T(1024)S(1)}, f32[1408]{0:T(1024)}, u32[]{:S(2)}) copy-start(f32[1408]{0:T(1024)} %param.31) | copy-start | bytes 16900
  337.5 9.5 %copy-start.14 = (f32[1408]{0:T(1024)S(1)}, f32[1408]{0:T(1024)}, u32[]{:S(2)}) copy-start(f32[1408]{0:T(1024)} %param.30) | copy-start | bytes 16900
  347.0 56.4 %copy-start.1 = (f32[1408,512]{1,0:T(8,128)S(1)}, f32[1408,512]{1,0:T(8,128)}, u32[]{:S(2)}) copy-start(f32[1408,512]{1,0:T(8,128)} %param.32) | copy-start | bytes 8650756
Sparse Core Ops, SparseCore 0:
  8.9 31.2 all-gather.11
  41.7 63.9 all-gather.19
  107.3 58.2 all-gather.17
  168.0 36.3 reduce-scatter.2
  205.8 59.0 all-gather.15
  266.4 27.1 all-gather.13
  364.3 36.6 reduce-scatter.4

commit v2 on v0

v2 whole, which is shorter than its diff:
```python
import functools

import jax
import jax.numpy as jnp
from jax import lax
from jax.experimental import pallas as pl
from jax.experimental.pallas import tpu as pltpu
from jax.sharding import PartitionSpec as P

MESH = pl.DeviceIdType.MESH
eps = 1e-06
H = 2
half_root = 0.7071067811865476


def gelu(a):
    return 0.5 * a * (1.0 + lax.erf(a * half_root))


def layer_kernel(
    dims,
    tokens,
    mix_gain,
    w_uv,
    w_mix,
    w_gate,
    w_up,
    w_down,
    u_scale,
    v_scale,
    spatial,
    bias,
    scales,
    ffn_gain,
    gate_scale,
    up_scale,
    out,
    uv_buf,
    mix_buf,
    gate_buf,
    up_buf,
    down_buf,
    scale_buf,
    tok_buf,
    res_buf,
    normed,
    gated,
    silu_buf,
    act,
    resid,
    give_buf,
    send_buf,
    pair_buf,
    far_buf,
    keep,
    z_send,
    z_recv,
    y_send,
    y_recv,
    w_local,
    s_send,
    s_recv,
    s_local,
    g_send,
    g_fwd,
    g_recv,
    g_local,
    p_send,
    p_recv,
    f_send,
    f_recv,
):
    n, n_tp = dims
    nx = n_tp // 2
    i = lax.axis_index("fs")
    g = lax.axis_index("grp")
    t = lax.axis_index("tp")
    x, c = t // 2, t % 2
    rows, dt = tokens.shape
    df = scales.shape[1]
    per = dt // df
    rt = rows // H
    partner = {"tp": x * 2 + 1 - c}
    across = {"grp": 1 - g}

    def remote(src, dst, ss, rs, device):
        return pltpu.make_async_remote_copy(
            src_ref=src,
            dst_ref=dst,
            send_sem=ss,
            recv_sem=rs,
            device_id=device,
            device_id_type=MESH,
        )

    barrier = pltpu.get_barrier_semaphore()
    for k in range(1, n):
        pl.semaphore_signal(barrier, 1, device_id={"fs": (i + k) % n}, device_id_type=MESH)
    pl.semaphore_signal(barrier, 1, device_id=across, device_id_type=MESH)
    pl.semaphore_signal(barrier, 1, device_id=partner, device_id_type=MESH)
    for k in range(1, nx):
        pl.semaphore_signal(
            barrier, 1, device_id={"tp": ((x + k) % nx) * 2 + c}, device_id_type=MESH
        )
    pl.semaphore_wait(barrier, (n - 1) + 2 + (nx - 1))

    cut = w_down.shape[0] // 2
    streams = (
        (w_uv, uv_buf, 0, w_uv.shape[0]),
        (w_mix, mix_buf, 0, w_mix.shape[0]),
        (w_gate, gate_buf, 0, w_gate.shape[0]),
        (w_up, up_buf, 0, w_up.shape[0]),
        (w_down, down_buf, 0, cut),
        (w_down, down_buf, cut, cut),
    )
    UV, MIX, GATE, UP, DOWN_A, DOWN_B = range(6)

    def part(k, who):
        half = streams[k][3] // 2
        return pl.ds(pl.multiple_of(streams[k][2] + who * half, 16), half)

    def z_copy(k, j, step, own):
        src, buf = streams[k][:2]
        sl = part(k, g)
        dst = buf.at[j, sl, :]
        slot = n if (own and step < 0) else j
        return remote(
            src.at[sl, :] if own else dst,
            dst,
            z_send.at[k, slot],
            z_recv.at[k, j],
            {"fs": jnp.clip(i + step, 0, n - 1)},
        )

    def y_copy(k, j, who):
        dst = streams[k][1].at[j, part(k, who), :]
        return remote(dst, dst, y_send.at[k, j], y_recv.at[k, j], across)

    def local_copy(k):
        src, buf, r0, count = streams[k]
        sl = pl.ds(r0, count)
        return pltpu.make_async_copy(src.at[sl, :], buf.at[i, sl, :], w_local.at[k])

    def own(k):
        @pl.when(i + 1 < n)
        def _():
            z_copy(k, i, 1, True).start()

        @pl.when(i > 0)
        def _():
            z_copy(k, i, -1, True).start()

    def service(k, s):
        left, right = i - s, i + s

        @pl.when(left >= 0)
        def _():
            z_copy(k, left, 1, False).wait_recv()

            @pl.when(i + 1 < n)
            def _():
                z_copy(k, left, 1, False).start()

            y_copy(k, left, g).start()

        @pl.when(right < n)
        def _():
            z_copy(k, right, -1, False).wait_recv()

            @pl.when(i > 0)
            def _():
                z_copy(k, right, -1, False).start()

            y_copy(k, right, g).start()

    def finish(k):
        local_copy(k).wait()
        for s in range(1, n):
            y_copy(k, lax.rem(i + s, n), 1 - g).wait_recv()

    def drain(k):
        @pl.when(i + 1 < n)
        def _():
            z_copy(k, i, 1, True).wait_send()

        @pl.when(i > 0)
        def _():
            z_copy(k, i, -1, True).wait_send()

        for s in range(1, n):
            j = lax.rem(i + s, n)
            y_copy(k, j, g).wait_send()

            @pl.when(jnp.logical_and(j < i, i + 1 < n))
            def _():
                z_copy(k, j, 1, False).wait_send()

            @pl.when(jnp.logical_and(j > i, i > 0))
            def _():
                z_copy(k, j, -1, False).wait_send()

    def scale_copy(s, mine):
        j = i if mine else lax.rem(i + s, n)
        return remote(
            scales,
            scale_buf.at[j],
            s_send.at[s],
            s_recv.at[j],
            {"fs": lax.rem(i + s, n)},
        )

    def chunk(h):
        return pl.ds(h * rt, rt)

    def far(k):
        return lax.rem(x + k, nx)

    def ag_x(r, src, buf, k, h):
        return remote(
            src.at[chunk(h), :],
            buf.at[t, chunk(h), :],
            g_send.at[r, k, h],
            g_recv.at[r, t, h],
            {"tp": far(k) * 2 + c} if k else partner,
        )

    def ag_in(r, buf, slot, h):
        ref = buf.at[slot, chunk(h), :]
        return remote(ref, ref, g_fwd.at[r, 0, h], g_recv.at[r, slot, h], partner)

    def ag_fwd(r, buf, k, h):
        slot = far(k) * 2 + c
        ref = buf.at[slot, chunk(h), :]
        return remote(ref, ref, g_fwd.at[r, k, h], g_recv.at[r, slot, h], partner)

    def ag_local(r, src, buf):
        return pltpu.make_async_copy(src, buf.at[t], g_local.at[r])

    def ag_start(r, src, buf):
        for h in range(H):
            for k in list(range(1, nx)) + [0]:
                ag_x(r, src, buf, k, h).start()
        ag_local(r, src, buf).start()

    def ag_finish(r, src, buf):
        for h in range(H):
            for k in range(1, nx):
                ag_fwd(r, buf, k, h).wait_recv()
                ag_fwd(r, buf, k, h).start()
        for h in range(H):
            for k in range(nx):
                ag_in(r, buf, far(k) * 2 + 1 - c, h).wait_recv()
        ag_local(r, src, buf).wait()

    def ag_drain(r, src, buf):
        for h in range(H):
            for k in range(nx):
                ag_x(r, src, buf, k, h).wait_send()
            for k in range(1, nx):
                ag_fwd(r, buf, k, h).wait_send()

    def norm(buf, gain):
        tile = 128

        def body(b, carry):
            sl = pl.ds(pl.multiple_of(b * tile, tile), tile)
            total = jnp.zeros((tile, 1), jnp.float32)
            for q in range(n_tp):
                wide = buf[q, sl, :].astype(jnp.float32)
                total = total + jnp.sum(wide * wide, axis=1, keepdims=True)
            factor = lax.rsqrt(total / (n_tp * dt) + eps)
            for q in range(n_tp):
                cols = slice(q * dt, (q + 1) * dt)
                wide = buf[q, sl, :].astype(jnp.float32)
                normed[sl, cols] = (wide * factor * gain[:, cols]).astype(jnp.bfloat16)
            return carry

        lax.fori_loop(0, rows // tile, body, 0)

    def pair_copy(r, xo, h):
        return remote(
            give_buf.at[xo, chunk(h), :],
            pair_buf.at[r, xo, chunk(h), :],
            p_send.at[r, xo, h],
            p_recv.at[r, xo, h],
            partner,
        )

    def far_copy(r, xo, h, slot):
        return remote(
            send_buf.at[xo, chunk(h), :],
            far_buf.at[r, slot, chunk(h), :],
            f_send.at[r, xo, h],
            f_recv.at[r, slot, h],
            {"tp": xo * 2 + c},
        )

    def reduce_over_tp(r, hidden, buf, scale_row, hook):
        def partial(owner, h):
            ws = [buf[owner * per + q] for q in range(per)]
            ss = [scale_buf[owner * per + q, scale_row : scale_row + 1, :] for q in range(per)]
            w = ws[0] if per == 1 else jnp.concatenate(ws, axis=1)
            s = ss[0] if per == 1 else jnp.concatenate(ss, axis=1)
            return jnp.dot(hidden[chunk(h), :], w, preferred_element_type=jnp.float32) * s

        for k in range(1, nx + 1):
            xo = far(k)
            for h in range(H):
                give_buf[xo, chunk(h), :] = partial(xo * 2 + 1 - c, h).astype(jnp.bfloat16)
                keep[xo, chunk(h), :] = partial(xo * 2 + c, h)
                pair_copy(r, xo, h).start()
            for h in range(H):
                pair_copy(r, xo, h).wait_recv()
                both = keep[xo, chunk(h), :] + pair_buf[r, xo, chunk(h), :].astype(jnp.float32)
                if k < nx:
                    send_buf[xo, chunk(h), :] = both.astype(jnp.bfloat16)
                else:
                    keep[xo, chunk(h), :] = both
            if k < nx:
                for h in range(H):
                    far_copy(r, xo, h, x).start()
        hook()

    def reduced(r, h):
        total = keep[x, chunk(h), :]
        for k in range(1, nx):
            far_copy(r, far(k), h, far(k)).wait_recv()
            total = total + far_buf[r, far(k), chunk(h), :].astype(jnp.float32)
        return total

    def reduce_drain(r):
        for k in range(1, nx + 1):
            for h in range(H):
                pair_copy(r, far(k), h).wait_send()
                if k < nx:
                    far_copy(r, far(k), h, x).wait_send()

    own(UV)
    own(MIX)
    ag_start(0, tokens, tok_buf)
    for s in range(1, n):
        scale_copy(s, True).start()
    own_scale = pltpu.make_async_copy(scales, scale_buf.at[i], s_local)
    own_scale.start()
    for k in range(6):
        local_copy(k).start()
    for s in range(1, n):
        service(UV, s)
        service(MIX, s)
    own(GATE)
    own(UP)
    ag_finish(0, tokens, tok_buf)
    norm(tok_buf, mix_gain)
    own_scale.wait()
    for s in range(1, n):
        scale_copy(s, False).wait_recv()
    finish(UV)

    groups, span = spatial.shape[0], spatial.shape[1]
    width = u_scale.shape[1]
    wide = width // groups
    causal = lax.broadcasted_iota(jnp.int32, (span, span), 0) >= lax.broadcasted_iota(
        jnp.int32, (span, span), 1
    )
    uv_w = uv_buf[...].reshape(-1, 2 * width)
    for h in range(H):
        pre = jnp.dot(normed[chunk(h), :], uv_w, preferred_element_type=jnp.float32)
        u = gelu(pre[:, :width] * u_scale[...])
        v = gelu(pre[:, width:] * v_scale[...]).astype(jnp.bfloat16)
        for q in range(groups):
            m = jnp.where(causal, spatial[q].astype(jnp.float32), 0.0).astype(jnp.bfloat16)
            cols = slice(q * wide, (q + 1) * wide)
            for b in range(rt // span):
                sl = slice(b * span, (b + 1) * span)
                mixed = jnp.dot(m, v[sl, cols], preferred_element_type=jnp.float32)
                mixed = mixed + bias[:, q : q + 1]
                gated[h * rt + b * span : h * rt + (b + 1) * span, cols] = (
                    u[sl, cols] * mixed
                ).astype(jnp.bfloat16)
    finish(MIX)

    def after_mix():
        service(GATE, 1)
        own(DOWN_A)

    reduce_over_tp(0, gated, mix_buf, 0, after_mix)
    for h in range(H):
        resid[chunk(h), :] = (
            tokens[chunk(h), :].astype(jnp.float32) + reduced(0, h)
        ).astype(jnp.bfloat16)
    ag_start(1, resid, res_buf)
    reduce_drain(0)
    for s in range(2, n):
        service(GATE, s)
    ag_finish(1, resid, res_buf)
    norm(res_buf, ffn_gain)
    for s in range(1, n):
        service(UP, s)
    own(DOWN_B)
    finish(GATE)


    ff = gate_scale.shape[1]
    gt = rows // 4

    def gate_step(b, carry):
        sl = pl.ds(pl.multiple_of(b * gt, 64), gt)
        a = jnp.dot(
            normed[sl, :], gate_buf[...].reshape(-1, ff), preferred_element_type=jnp.float32
        )
        a = a * gate_scale[...]
        silu_buf[sl, :] = a / (1.0 + jnp.exp(-a))
        return carry

    lax.fori_loop(0, 4, gate_step, 0)
    for s in range(1, n):
        service(DOWN_A, s)
    finish(UP)

    def up_step(b, carry):
        sl = pl.ds(pl.multiple_of(b * gt, 64), gt)
        a = jnp.dot(
            normed[sl, :], up_buf[...].reshape(-1, ff), preferred_element_type=jnp.float32
        )
        act[sl, :] = (silu_buf[sl, :] * (a * up_scale[...])).astype(jnp.bfloat16)
        return carry

    lax.fori_loop(0, 4, up_step, 0)
    for s in range(1, n):
        service(DOWN_B, s)
    finish(DOWN_A)
    finish(DOWN_B)
    reduce_over_tp(1, act, down_buf, 8, lambda: None)
    for h in range(H):
        out[chunk(h), :] = (
            resid[chunk(h), :].astype(jnp.float32) + reduced(1, h)
        ).astype(jnp.bfloat16)
    reduce_drain(1)
    ag_drain(0, tokens, tok_buf)
    ag_drain(1, resid, res_buf)
    for k in range(6):
        drain(k)
    for s in range(1, n):
        scale_copy(s, True).wait_send()


def local(
    dims,
    tokens,
    mix_gain,
    w_u,
    w_v,
    u_scale,
    v_scale,
    spatial,
    spatial_bias,
    w_mix,
    mix_scale,
    ffn_gain,
    w_gate,
    w_up,
    gate_scale,
    up_scale,
    w_down,
    down_scale,
):
    n, n_tp = dims
    nx = n_tp // 2
    half = jnp.bfloat16
    rows, dt = tokens.shape
    df = mix_scale.shape[1]
    scales = jnp.concatenate(
        [jnp.broadcast_to(mix_scale, (8, df)), jnp.broadcast_to(down_scale, (8, df))], axis=0
    )
    w_uv = jnp.concatenate([w_u, w_v], axis=1).astype(half)
    hbm = pl.BlockSpec(memory_space=pl.ANY)
    vmem = pl.BlockSpec(memory_space=pltpu.VMEM)
    ff = w_gate.shape[1]
    dma = pltpu.SemaphoreType.DMA
    return pl.pallas_call(
        functools.partial(layer_kernel, dims),
        out_shape=jax.ShapeDtypeStruct((rows, dt), half),
        in_specs=[vmem, vmem] + [hbm] * 5 + [vmem] * 8,
        out_specs=vmem,
        scratch_shapes=[
            pltpu.VMEM((n,) + w_uv.shape, half),
            pltpu.VMEM((n,) + w_mix.shape, half),
            pltpu.VMEM((n,) + w_gate.shape, half),
            pltpu.VMEM((n,) + w_up.shape, half),
            pltpu.VMEM((n,) + w_down.shape, half),
            pltpu.VMEM((n,) + scales.shape, jnp.float32),
            pltpu.VMEM((n_tp, rows, dt), half),
            pltpu.VMEM((n_tp, rows, dt), half),
            pltpu.VMEM((rows, n_tp * dt), half),
            pltpu.VMEM((rows, w_u.shape[1]), half),
            pltpu.VMEM((rows, ff), jnp.float32),
            pltpu.VMEM((rows, ff), half),
            pltpu.VMEM((rows, dt), half),
            pltpu.VMEM((nx, rows, dt), half),
            pltpu.VMEM((nx, rows, dt), half),
            pltpu.VMEM((2, nx, rows, dt), half),
            pltpu.VMEM((2, nx, rows, dt), half),
            pltpu.VMEM((nx, rows, dt), jnp.float32),
            dma((6, n + 1)),
            dma((6, n)),
            dma((6, n)),
            dma((6, n)),
            dma((6,)),
            dma((n,)),
            dma((n,)),
            dma,
            dma((2, nx, H)),
            dma((2, nx, H)),
            dma((2, n_tp, H)),
            dma((2,)),
            dma((2, nx, H)),
            dma((2, nx, H)),
            dma((2, nx, H)),
            dma((2, nx, H)),
        ],
        compiler_params=pltpu.CompilerParams(
            collective_id=0, has_side_effects=True, vmem_limit_bytes=66000000
        ),
    )(
        tokens,
        mix_gain[None],
        w_uv,
        w_mix.astype(half),
        w_gate.astype(half),
        w_up.astype(half),
        w_down.astype(half),
        u_scale[None],
        v_scale[None],
        spatial,
        spatial_bias.T,
        scales,
        ffn_gain[None],
        gate_scale[None],
        up_scale[None],
    )


def solution(mesh):
    placed = (
        P(("grp", "fs"), "tp"),
        P(),
        P("fs", "tp"),
        P("fs", "tp"),
        P("tp"),
        P("tp"),
        P("tp", None, None),
        P("tp", None),
        P("tp", "fs"),
        P(None, "fs"),
        P(),
        P("fs", "tp"),
        P("fs", "tp"),
        P("tp"),
        P("tp"),
        P("tp", "fs"),
        P(None, "fs"),
    )
    dims = (mesh.shape["fs"], mesh.shape["tp"])
    return jax.shard_map(
        functools.partial(local, dims),
        mesh=mesh,
        in_specs=placed,
        out_specs=P(("grp", "fs"), "tp"),
        check_vma=False,
    )
```

time: 589 us -> 257 us (0.44)
  waiting for transfers between devices: 480 us -> 0 us
  Pallas kernels: 0 us -> 239 us
  matrix products: 43 us -> 0 us
  blocking collectives: 25.8 us -> 0 us
  between operations: 13.6 us -> 0.03 us
  other arithmetic: 22.3 us -> 9.43 us
    all_gather x8 -> x0, waiting for transfers between devices: 406 us -> none  [the longest x2 135 us: collect_out(): lax.all_gather(weight.astype(jnp.bfloat16), 'fs', axis=1, tiled=True)]
    pallas_call x0 -> x1, Pallas kernels: none -> 239 us  [local(): pl.pallas_call(functools.partial(layer_kernel, dims), out_shape=jax.Shape...]
    reduce_scatter x2 -> x0, waiting for transfers between devices: 73.3 us -> none  [reduce_out(): lax.psum_scatter(term.astype(jnp.bfloat16), 'tp', scatter_dimension=1, ti...]
    dot_general x5 -> x0, matrix products: 43 us -> none  [the longest x2 25.5 us: reduce_out(): term = jnp.dot(hidden, weight, preferred_element_type=jnp.float32) * scale]
    all_gather x2 -> x0, blocking collectives: 25.8 us -> none  [collect_out(): lax.all_gather(scale.astype(jnp.bfloat16), 'fs', axis=1, tiled=True)]
    convert_element_type x10 -> x4, other arithmetic: 16.6 us -> 5.84 us  [the longest x1 1.99 us: local(): w_mix.astype(half)]
  transfers between devices with their start and end apart: 10 -> 0, of which waited for: 10 -> 0; matrix products, arithmetic and copies ran while one was open for 7% -> 0% of each run, Pallas kernels for 0% -> 0%
where the time goes in v2:
time: 257 us
  Pallas kernels  239 us (93%)
  other arithmetic  9.43 us (4%)
  local copies, waits for them, and re-layouts  8.65 us (3%)
    pallas_call x1, Pallas kernels, local(): pl.pallas_call(functools.partial(layer_kernel, dims), out_shape=jax.Shape...  239 us

profile of v2, /device:TPU:0, one launch (start us, length us, event | category | flops | bytes accessed | tf_op | source)
XLA Modules:
  0.0 256.6 jit_solution(14437769824699149306)
XLA Ops:
  0.0 0.0 copy-start
  0.0 1.4 broadcast_in_dim.40.gate_scale
  1.4 1.3 broadcast_in_dim.41.up_scale
  2.7 0.7 broadcast_in_dim.36
  3.4 0.7 broadcast_in_dim.38
  4.1 0.6 pad_maximum_fusion.1.scales
  4.7 1.4 copy.18
  6.1 1.1 convert.6
  7.2 1.1 convert.7
  8.3 0.0 copy-start.1
  8.3 0.8 pad_maximum_fusion.w_uv
  9.1 2.0 convert_element_type.13.w_mix
  11.1 0.0 copy-done
  11.1 1.3 convert_element_type.14.w_gate
  12.4 0.0 copy-done.1
  12.4 0.0 copy-start.2
  12.4 1.3 convert_element_type.15.w_up
  13.7 1.1 copy-done.2
  14.7 1.3 convert_element_type.16.w_down
  16.0 238.5 %shard_map.163 = bf16[768,512]{1,0:T(8,128)(2,1)} custom-call(bf16[768,512]{1,0:T(8,128)(2,1)} %tokens.1, f32[1,2048]{1,0:T(1,128)} %bitcast.8, bf16[512,512]{1,0:T(8,128)(2,1)} %pad_maximum_fusion.w_uv, bf16[256,512]{1,0:T(8,128)(2,1)} %convert_element_type.13.w_mix, bf16[512,1408]{1,0:T(8,128)(2,1)} %convert_element_type.14.w_gate, ...), custom_call_target="tpu_custom_call" | custom-call | tf_op jit(solution)/shard_map/pallas_call | solution.py:480
  254.6 2.1 copy.20
Async XLA Ops:
  0.0 11.1 %copy-start = (f32[512,1408]{1,0:T(8,128)S(1)}, f32[512,1408]{1,0:T(8,128)}, u32[]{:S(2)}) copy-start(f32[512,1408]{1,0:T(8,128)} %param.28) | copy-start | bytes 8650756
  8.3 4.1 %copy-start.1 = (f32[512,1408]{1,0:T(8,128)S(1)}, f32[512,1408]{1,0:T(8,128)}, u32[]{:S(2)}) copy-start(f32[512,1408]{1,0:T(8,128)} %param.29) | copy-start | bytes 8650756
  12.4 2.3 copy-start.2

commit v3 on v2

--- a/solution.py
+++ b/solution.py
@@ -20,20 +20,17 @@
 def layer_kernel(
     dims,
     tokens,
-    mix_gain,
+    gains,
     w_uv,
     w_mix,
     w_gate,
     w_up,
     w_down,
-    u_scale,
-    v_scale,
+    uv_scale,
     spatial,
     bias,
     scales,
-    ffn_gain,
-    gate_scale,
-    up_scale,
+    ffn_scale,
     out,
     uv_buf,
     mix_buf,
@@ -104,16 +101,17 @@
         )
     pl.semaphore_wait(barrier, (n - 1) + 2 + (nx - 1))
 
-    cut = w_down.shape[0] // 2
+    units = w_down.shape[0] // 32
+    first = units // 2
+    second = (units - first + 1) // 2
+    ends = (0, first * 32, (first + second) * 32, w_down.shape[0])
     streams = (
         (w_uv, uv_buf, 0, w_uv.shape[0]),
         (w_mix, mix_buf, 0, w_mix.shape[0]),
         (w_gate, gate_buf, 0, w_gate.shape[0]),
         (w_up, up_buf, 0, w_up.shape[0]),
-        (w_down, down_buf, 0, cut),
-        (w_down, down_buf, cut, cut),
-    )
-    UV, MIX, GATE, UP, DOWN_A, DOWN_B = range(6)
+    ) + tuple((w_down, down_buf, ends[q], ends[q + 1] - ends[q]) for q in range(3))
+    UV, MIX, GATE, UP, DOWN_A, DOWN_B, DOWN_C = range(7)
 
     def part(k, who):
         half = streams[k][3] // 2
@@ -172,6 +170,10 @@
                 z_copy(k, right, -1, False).start()
 
             y_copy(k, right, g).start()
+
+    def run(k, begin, end):
+        for s in range(begin, min(end, n)):
+            service(k, s)
 
     def finish(k):
         local_copy(k).wait()
@@ -342,38 +344,40 @@
         scale_copy(s, True).start()
     own_scale = pltpu.make_async_copy(scales, scale_buf.at[i], s_local)
     own_scale.start()
-    for k in range(6):
+    for k in range(7):
         local_copy(k).start()
     for s in range(1, n):
         service(UV, s)
         service(MIX, s)
-    own(GATE)
-    own(UP)
+        if s == max(n - 2, 1):
+            own(GATE)
+            own(UP)
     ag_finish(0, tokens, tok_buf)
-    norm(tok_buf, mix_gain)
+    norm(tok_buf, gains[0:1, :])
     own_scale.wait()
     for s in range(1, n):
         scale_copy(s, False).wait_recv()
     finish(UV)
 
     groups, span = spatial.shape[0], spatial.shape[1]
-    width = u_scale.shape[1]
+    width = uv_scale.shape[1]
     wide = width // groups
     causal = lax.broadcasted_iota(jnp.int32, (span, span), 0) >= lax.broadcasted_iota(
         jnp.int32, (span, span), 1
     )
     uv_w = uv_buf[...].reshape(-1, 2 * width)
+    tilt = [jnp.broadcast_to(bias[q : q + 1, :], (span, span)).T[:, :1] for q in range(groups)]
     for h in range(H):
         pre = jnp.dot(normed[chunk(h), :], uv_w, preferred_element_type=jnp.float32)
-        u = gelu(pre[:, :width] * u_scale[...])
-        v = gelu(pre[:, width:] * v_scale[...]).astype(jnp.bfloat16)
+        u = gelu(pre[:, :width] * uv_scale[0:1, :])
+        v = gelu(pre[:, width:] * uv_scale[1:2, :]).astype(jnp.bfloat16)
         for q in range(groups):
             m = jnp.where(causal, spatial[q].astype(jnp.float32), 0.0).astype(jnp.bfloat16)
             cols = slice(q * wide, (q + 1) * wide)
             for b in range(rt // span):
                 sl = slice(b * span, (b + 1) * span)
                 mixed = jnp.dot(m, v[sl, cols], preferred_element_type=jnp.float32)
-                mixed = mixed + bias[:, q : q + 1]
+                mixed = mixed + tilt[q]
                 gated[h * rt + b * span : h * rt + (b + 1) * span, cols] = (
                     u[sl, cols] * mixed
                 ).astype(jnp.bfloat16)
@@ -390,17 +394,20 @@
         ).astype(jnp.bfloat16)
     ag_start(1, resid, res_buf)
     reduce_drain(0)
-    for s in range(2, n):
-        service(GATE, s)
+    run(UP, 1, 2)
+    run(GATE, 2, 3)
+    own(DOWN_B)
     ag_finish(1, resid, res_buf)
-    norm(res_buf, ffn_gain)
-    for s in range(1, n):
-        service(UP, s)
-    own(DOWN_B)
+    norm(res_buf, gains[1:2, :])
+    run(UP, 2, 3)
+    run(GATE, 3, n)
+    own(DOWN_C)
+    run(DOWN_A, 1, 2)
+    run(DOWN_B, 1, 2)
     finish(GATE)
 
 
-    ff = gate_scale.shape[1]
+    ff = ffn_scale.shape[1]
     gt = rows // 4
 
     def gate_step(b, carry):
@@ -408,13 +415,15 @@
         a = jnp.dot(
             normed[sl, :], gate_buf[...].reshape(-1, ff), preferred_element_type=jnp.float32
         )
-        a = a * gate_scale[...]
+        a = a * ffn_scale[0:1, :]
         silu_buf[sl, :] = a / (1.0 + jnp.exp(-a))
         return carry
 
     lax.fori_loop(0, 4, gate_step, 0)
-    for s in range(1, n):
-        service(DOWN_A, s)
+    run(UP, 3, n)
+    run(DOWN_C, 1, 2)
+    run(DOWN_A, 2, 3)
+    run(DOWN_B, 2, 3)
     finish(UP)
 
     def up_step(b, carry):
@@ -422,14 +431,17 @@
         a = jnp.dot(
             normed[sl, :], up_buf[...].reshape(-1, ff), preferred_element_type=jnp.float32
         )
-        act[sl, :] = (silu_buf[sl, :] * (a * up_scale[...])).astype(jnp.bfloat16)
+        act[sl, :] = (silu_buf[sl, :] * (a * ffn_scale[1:2, :])).astype(jnp.bfloat16)
         return carry
 
     lax.fori_loop(0, 4, up_step, 0)
-    for s in range(1, n):
-        service(DOWN_B, s)
+    run(DOWN_C, 2, 3)
+    run(DOWN_A, 3, n)
+    run(DOWN_B, 3, n)
+    run(DOWN_C, 3, n)
     finish(DOWN_A)
     finish(DOWN_B)
+    finish(DOWN_C)
     reduce_over_tp(1, act, down_buf, 8, lambda: None)
     for h in range(H):
         out[chunk(h), :] = (
@@ -438,7 +450,7 @@
     reduce_drain(1)
     ag_drain(0, tokens, tok_buf)
     ag_drain(1, resid, res_buf)
-    for k in range(6):
+    for k in range(7):
         drain(k)
     for s in range(1, n):
         scale_copy(s, True).wait_send()
@@ -480,7 +492,7 @@
     return pl.pallas_call(
         functools.partial(layer_kernel, dims),
         out_shape=jax.ShapeDtypeStruct((rows, dt), half),
-        in_specs=[vmem, vmem] + [hbm] * 5 + [vmem] * 8,
+        in_specs=[vmem, vmem] + [hbm] * 5 + [vmem] * 5,
         out_specs=vmem,
         scratch_shapes=[
             pltpu.VMEM((n,) + w_uv.shape, half),
@@ -501,11 +513,11 @@
             pltpu.VMEM((2, nx, rows, dt), half),
             pltpu.VMEM((2, nx, rows, dt), half),
             pltpu.VMEM((nx, rows, dt), jnp.float32),
-            dma((6, n + 1)),
-            dma((6, n)),
-            dma((6, n)),
-            dma((6, n)),
-            dma((6,)),
+            dma((7, n + 1)),
+            dma((7, n)),
+            dma((7, n)),
+            dma((7, n)),
+            dma((7,)),
             dma((n,)),
             dma((n,)),
             dma,
@@ -523,20 +535,17 @@
         ),
     )(
         tokens,
-        mix_gain[None],
+        jnp.stack([mix_gain, ffn_gain]),
         w_uv,
         w_mix.astype(half),
         w_gate.astype(half),
         w_up.astype(half),
         w_down.astype(half),
-        u_scale[None],
-        v_scale[None],
+        jnp.stack([u_scale, v_scale]),
         spatial,
-        spatial_bias.T,
+        spatial_bias,
         scales,
-        ffn_gain[None],
-        gate_scale[None],
-        up_scale[None],
+        jnp.stack([gate_scale, up_scale]),
     )
 
 

time: 257 us -> 243 us (0.946)
  Pallas kernels: 239 us -> 223 us
  other arithmetic: 9.43 us -> 12.8 us
  local copies, waits for them, and re-layouts: 8.65 us -> 5.92 us
    pallas_call x1, Pallas kernels: 239 us -> 223 us  [local(): pl.pallas_call(functools.partial(layer_kernel, dims), out_shape=jax.Shape...]
    another operation x2 -> x5, other arithmetic: 2.14 us -> 5.49 us
    broadcast_in_dim x2 -> x0, local copies, waits for them, and re-layouts: 2.73 us -> none  [the longest x1 1.44 us: local(): gate_scale[None]]
where the time goes in v3:
time: 243 us; the launch traced here: 242 us
  Pallas kernels  223 us (92%)
  other arithmetic  12.8 us (5%)
  local copies, waits for them, and re-layouts  5.92 us (2%)
    pallas_call x1, Pallas kernels, local(): pl.pallas_call(functools.partial(layer_kernel, dims), out_shape=jax.Shape...  223 us

profile of v3, /device:TPU:0, one launch (start us, length us, event | category | flops | bytes accessed | tf_op | source)
XLA Modules:
  0.0 242.0 jit_solution(8783871315519701852)
XLA Ops:
  0.0 0.0 copy-start
  0.0 1.4 pad_maximum_fusion.4.uv_scale
  1.4 0.7 stack.33
  2.1 0.7 stack.34
  2.8 0.6 pad_maximum_fusion.3.ffn_scale
  3.4 1.3 pad_maximum_fusion.2.gains
  4.8 0.7 broadcast_in_dim.15
  5.4 0.7 broadcast_in_dim.17
  6.1 0.6 pad_maximum_fusion.1.scales
  6.7 1.1 convert.6
  7.8 1.1 convert.7
  8.9 0.0 copy-start.1
  8.9 0.8 pad_maximum_fusion.w_uv
  9.7 2.0 convert_element_type.13.w_mix
  11.7 0.0 copy-done
  11.7 1.3 convert_element_type.14.w_gate
  13.0 0.0 copy-done.1
  13.0 0.0 copy-start.2
  13.0 1.3 convert_element_type.15.w_up
  14.3 1.1 copy-done.2
  15.3 1.3 convert_element_type.16.w_down
  16.7 223.2 %shard_map.163 = bf16[768,512]{1,0:T(8,128)(2,1)} custom-call(bf16[768,512]{1,0:T(8,128)(2,1)} %tokens.1, f32[2,2048]{1,0:T(2,128)} %pad_maximum_fusion.2.gains, bf16[512,512]{1,0:T(8,128)(2,1)} %pad_maximum_fusion.w_uv, bf16[256,512]{1,0:T(8,128)(2,1)} %convert_element_type.13.w_mix, bf16[512,1408]{1,0:T(8,128)(2,1)} %convert_element_type.14.w_gate, ...), custom_call_target="tpu_custom_call" | custom-call | tf_op jit(solution)/shard_map/pallas_call | solution.py:492
  239.9 2.1 copy.19
Async XLA Ops:
  0.0 11.7 %copy-start = (f32[512,1408]{1,0:T(8,128)S(1)}, f32[512,1408]{1,0:T(8,128)}, u32[]{:S(2)}) copy-start(f32[512,1408]{1,0:T(8,128)} %param.28) | copy-start | bytes 8650756
  8.9 4.1 %copy-start.1 = (f32[512,1408]{1,0:T(8,128)S(1)}, f32[512,1408]{1,0:T(8,128)}, u32[]{:S(2)}) copy-start(f32[512,1408]{1,0:T(8,128)} %param.29) | copy-start | bytes 8650756
  13.0 2.3 copy-start.2
